TPU v7x, 512 devices: a whole 4x8x8 slice. The times are simulated.
512 devices in a mesh: sp: 64 (over z, y), fs: 4 (over x), tp: 2 (over core).
Axes of the slice: x: 4, y: 8, z: 8, core: 2. Of those that a mesh axis runs over, the one named last changes fastest.
Arguments:
- tokens: bfloat16 [4, 8192, 2048], P('fs', ('sp', 'tp')), may hold values from -6 to 6
- norm_gain: float32 [2048], replicated, may hold values from 0.1 to 1.9
- rec_query: bfloat16 [2048, 512], P('sp', 'tp'), may hold values from -0.125 to 0.125
- rec_input: bfloat16 [2048, 512], P('sp', 'tp'), may hold values from -0.125 to 0.125
- rec_forward: bfloat16 [2048, 512], P('sp', 'tp'), may hold values from -0.125 to 0.125
- rec_backward: bfloat16 [2048, 512], P('sp', 'tp'), may hold values from -0.125 to 0.125
- forget_gap: float32 [2, 512], P(None, 'tp'), may hold values from 0 to 0.06
- log_decay: float32 [4, 2, 4, 8192], P('fs', None, 'tp', 'sp'), may hold values from -0.7 to 0
- rec_gain: float32 [512], P('tp'), may hold values from 0.1 to 1.9
- conv_value: bfloat16 [2048, 512], P('sp', 'tp'), may hold values from -0.125 to 0.125
- conv_gate: bfloat16 [2048, 512], P('sp', 'tp'), may hold values from -0.125 to 0.125
- conv_kernel: bfloat16 [31, 512], P(None, 'tp'), may hold values from -3.1 to 3.1
- conv_gain: float32 [512], P('tp'), may hold values from 0.1 to 1.9
- out_rec: bfloat16 [512, 2048], P('tp', 'sp'), may hold values from -0.1875 to 0.1875
- out_conv: bfloat16 [512, 2048], P('tp', 'sp'), may hold values from -0.1875 to 0.1875
Outputs:
- mixed: bfloat16 [4, 8192, 2048], P('fs', ('sp', 'tp'))
All inputs are finite; a program needn't handle non-finite values.
Results may differ from a plain program's by a relative error of at most 0.017.
Values may be sent and summed in bfloat16 or wider, within the bound.
No kernel may reach another device: no remote copies, remote signals or barrier semaphores. Data moves between devices by JAX's collectives and lax.ppermute only.
A program may use at most 64 MiB of HBM per device.

v0:
```python
import jax
import jax.numpy as jnp
from jax import lax
from jax.experimental import pallas as pl
from jax.experimental.pallas import tpu as pltpu
from jax.sharding import Mesh
from jax.sharding import PartitionSpec as P

KD = 128
BLOCK = 64
TILE = 512
SMALL = pltpu.CompilerParams(vmem_limit_bytes=24 * 1024 * 1024)
EPS = 1e-06
Z, Y, X, C = "sp_0", "sp_1", "fs", "tp"
F32, BF16 = jnp.float32, jnp.bfloat16
NN = (((1,), (0,)), ((), ()))
NT = (((1,), (1,)), ((), ()))
TN = (((0,), (0,)), ((), ()))


def dot(a, b, dims):
    return lax.dot_general(a, b, dims, preferred_element_type=F32)


def sigmoid(x):
    return 1.0 / (1.0 + jnp.exp(-x))


def lanes(rows):
    return lax.broadcasted_iota(jnp.int32, (rows, 128), 1)


def triangles():
    r = lax.broadcasted_iota(jnp.int32, (128, 128), 0)
    c = lax.broadcasted_iota(jnp.int32, (128, 128), 1)
    same = (r // BLOCK) == (c // BLOCK)
    return same & (c <= r), same & (c >= r)


def split_dot(mask, x):
    hi = x.astype(BF16)
    lo = (x - hi.astype(F32)).astype(BF16)
    return dot(mask, jnp.concatenate([hi, lo], axis=0), NN)


def project(x_ref, w_ref, rows, width):
    acc = jnp.zeros((rows.stop - rows.start, width), F32)
    for k in range(8):
        acc += dot(x_ref[rows, 256 * k : 256 * (k + 1)], w_ref[k], NT)
    return acc


def rounded(acc):
    return acc.astype(BF16).astype(F32)


def gate_keys(a, gap):
    return gap * sigmoid(-a)


def start_kernel(
    x_ref, gain_ref, rf_ref, rb_ref, rq_ref, cv_ref, cg_ref, ri_ref, ld_ref, rec_ref, conv_ref,
    norm_ref, out_ref,
):
    for r in range(0, 64, 16):
        x = x_ref[r : r + 16, :].astype(F32)
        scale = lax.rsqrt(jnp.mean(x * x, axis=1, keepdims=True) + EPS)
        norm_ref[r : r + 16, :] = (x * scale * gain_ref[...]).astype(BF16)
    group = lanes(32) // 32
    row = lax.broadcasted_iota(jnp.int32, (32, 128), 0)
    for m in range(2):
        cols = slice(128 * m, 128 * (m + 1))
        src = [r[:, cols].astype(F32) for r in (rf_ref, rb_ref, rq_ref, ri_ref)]
        value_c = cv_ref[:, cols].astype(F32)
        gate_c = cg_ref[:, cols].astype(F32)
        decays = jnp.zeros((32, 128), F32)
        for d in range(2):
            rest = jnp.broadcast_to(ld_ref[d, m : m + 1, :], (8, 128))
            for s in range(3):
                part = rest.astype(BF16).astype(F32)
                rest = rest - part
                low = pltpu.roll(part, 64, 1)[0:1]
                decays = jnp.where(row == 2 * s + d, low, decays)
                decays = jnp.where(row == 6 + 2 * s + d, part[0:1], decays)
        turned = [pltpu.roll(x, 64, 1) for x in src]
        for q in range(4):
            y = 4 * m + q
            keys, values = q // 2, q % 2
            fwd = turned[0] if keys else src[0]
            bwd = src[1] if keys else turned[1]
            query = turned[2] if keys else src[2]
            value = turned[3] if values else src[3]
            conv = pltpu.roll(value_c, (32 * (2 - q)) % 128, 1) if q != 2 else value_c
            gate = pltpu.roll(gate_c, (32 * (3 - q)) % 128, 1) if q != 3 else gate_c
            value = jnp.where(group < 2, value, jnp.where(group == 2, conv, gate))
            out_ref[y, :, 0:128] = jnp.where(group < 2, fwd, bwd).astype(BF16)
            out_ref[y, :, 128:256] = value.astype(BF16)
            out_ref[y, :, 256:384] = jnp.where(group < 2, query, decays).astype(BF16)
            out_ref[y, :, 384:640] = rec_ref[...]
            out_ref[y, :, 640:896] = conv_ref[...]


def second_kernel(
    first_ref, gap_ref, taps_ref, w_ref, w2_ref, cols_ref, ld_ref, gap_out, taps_out
):
    gap_out[...] = gap_ref[...]
    taps_out[...] = taps_ref[...]
    lane = lanes(8)
    tiles = [[], [], []]
    for y in range(8):
        for t in range(3):
            tiles[t].append(first_ref[y, :, 128 * t : 128 * (t + 1)].astype(F32))
        third = tiles[2][-1]
        cols_ref[32 * y : 32 * (y + 1), :] = first_ref[y, :, 384:896]
        low = third[0:2] + third[2:4] + third[4:6]
        high = third[6:8] + third[8:10] + third[10:12]
        low = jnp.concatenate([low, low, low, low], axis=0)
        high = jnp.concatenate([high, high, high, high], axis=0)
        ld_ref[y] = jnp.where(lane < 64, pltpu.roll(low, 64, 1), high)[0:2]
    keys, values, queries = [jnp.concatenate(t, axis=0).T.astype(BF16) for t in tiles]
    w_ref[0:128, :] = keys
    w_ref[128:224, :] = values[0:96]
    w_ref[224:248, :] = queries[0:24]
    for i in range(8):
        w2_ref[i, 0:32, :] = values[96:128]
        w2_ref[i, 32:72, :] = queries[24:64]


def states_kernel(
    z_ref, x_hbm, w_ref, w2_ref, ld_ref, gap_ref,
    a_ref, v_ref, c_ref, send_ref, before_ref, offset_ref,
    x_ref, sems, chunk_s, chunk_t,
):
    z = z_ref[0]
    rows = TILE
    total = x_ref.shape[0]
    n = total // 64
    copies = []
    for t in range(total // rows):
        at = pl.ds(rows * t, rows)
        copies.append(pltpu.make_async_copy(x_hbm.at[at], x_ref.at[at], sems.at[t]))
        copies[-1].start()
    lower, upper = triangles()
    lower_f, upper_f = lower.astype(F32), upper.astype(F32)
    lower_b = lower_f.astype(BF16)
    lower_b = jnp.concatenate([lower_b, lower_b], axis=1)
    lane = lanes(128)
    lane1 = lanes(1)

    def gates(b):
        at = slice(128 * b, 128 * (b + 1))
        a = a_ref[at, :].astype(F32)
        v = v_ref[at, 0:64]
        k = gate_keys(a, gap_ref[...])
        g = jnp.log1p(-k)
        ld = ld_ref[b]
        sums = split_dot(lower_b, g)
        first, second = sums[63:64], sums[127:128]
        ends = jnp.concatenate(
            [jnp.broadcast_to(first, (64, 128)), jnp.broadcast_to(second, (64, 128))], axis=0
        )
        cum_f = sums + jnp.sum(lower_f * ld[0:1], axis=1, keepdims=True)
        cum_b = ends - sums + g + jnp.sum(upper_f * ld[1:2], axis=1, keepdims=True)
        cum = jnp.where(lane < 64, cum_f, cum_b)
        c_ref[at, :] = cum
        for h in range(2):
            part = slice(64 * h, 64 * (h + 1))
            cc = cum[part]
            tot = jnp.where(lane1 < 64, cc[63:64], cc[0:1])
            kd = (k[part] * jnp.exp(tot - cc)).astype(BF16)
            chunk_s[2 * b + h] = dot(v[part], kd, TN)
            chunk_t[2 * b + h] = jnp.broadcast_to(tot, (8, 128))

    for t, copy in enumerate(copies):
        copy.wait()
        at = slice(rows * t, rows * (t + 1))
        acc = project(x_ref, w_ref, at, 248)
        if t:
            for b in range(rows // 128):
                gates((t - 1) * (rows // 128) + b)
        a_ref[at, :] = acc[:, :128].astype(BF16)
        v_ref[at, :] = jnp.concatenate([acc[:, 128:], jnp.zeros((rows, 8), F32)], axis=1).astype(BF16)
    ends = []
    for at in (slice(0, 16), slice(total - 16, total)):
        gate = rounded(project(x_ref, w2_ref, at, 72)[:, 0:32])
        ends.append(v_ref[at, :].astype(F32)[:, 64:96] * sigmoid(gate))
    head, last = ends
    for b in range(total // 128 - rows // 128, total // 128):
        gates(b)

    fwd = lanes(64) < 64
    fwd8 = lanes(8) < 64
    s = jnp.zeros((64, 128), F32)
    off = jnp.zeros((8, 128), F32)
    befores, offs = [None] * n, [None] * n
    for i in range(n):
        j = n - 1 - i
        befores[i], offs[i] = s, off
        tt = jnp.where(fwd8, chunk_t[i], chunk_t[j])
        sc = jnp.where(fwd, chunk_s[i], chunk_s[j])
        s = s * jnp.exp(tt)[0:1] + sc
        off = off + tt
        if i >= n // 2:
            for p, q in ((i, j), (j, i)):
                before_ref[p] = jnp.where(fwd, befores[p], befores[q]).astype(BF16)
                offset_ref[p] = jnp.where(fwd8, offs[p], offs[q])
    dec = jnp.exp(off)
    hi = dec.astype(BF16).astype(F32)
    lo = dec - hi
    fwd32 = lanes(32) < 64
    later = jnp.where(fwd32, s[0:32], pltpu.roll(s[32:64], 64, 1))
    earlier = jnp.where(fwd32, pltpu.roll(s[0:32], 64, 1), s[32:64])
    row = lax.broadcasted_iota(jnp.int32, (16, 128), 0)
    edge = jnp.concatenate([head, last, last, last], axis=1)

    def with_decay(hi, lo):
        return jnp.where(lanes(16) < 64, edge, jnp.where(row == 0, hi[0:1], lo[0:1]))

    later_tail = with_decay(pltpu.roll(hi, 64, 1), pltpu.roll(lo, 64, 1))
    earlier_tail = with_decay(hi, lo)
    for i in range(8):
        ahead = jnp.where(i > z, 1, 0) > 0
        send_ref[i, 0:32, :] = jnp.where(ahead, later, earlier).astype(BF16)
        send_ref[i, 32:48, :] = jnp.where(ahead, later_tail, earlier_tail).astype(BF16)


def local_kernel(
    x_hbm, w2_ref, a_ref, v_ref, c_ref, gap_ref, before_ref, offset_ref, taps_ref,
    out_ref, qd_ref, conv_ref, edge_ref, x_ref, sems, pad,
):
    n = x_ref.shape[0]
    copies = []
    for t in range(n // TILE):
        at = pl.ds(TILE * t, TILE)
        copies.append(pltpu.make_async_copy(x_hbm.at[at], x_ref.at[at], sems.at[t]))
        copies[-1].start()
    lower, upper = triangles()
    lane = lanes(128)
    zeros = jnp.zeros((16, 32), F32)
    pad[0:16, :] = zeros
    for b in range(n // 128):
        rows = slice(128 * b, 128 * (b + 1))
        if b % (TILE // 128) == 0:
            t = b // (TILE // 128)
            copies[t].wait()
            late = rounded(project(x_ref, w2_ref, slice(TILE * t, TILE * (t + 1)), 72))
        extra = late[128 * b - TILE * t : 128 * (b + 1) - TILE * t]
        mixed = v_ref[rows, :].astype(F32)
        v = v_ref[rows, 0:64]
        gated = mixed[:, 64:96] * sigmoid(extra[:, 0:32])
        pad[16 + 128 * b : 16 + 128 * (b + 1), :] = rounded(gated)
        a = a_ref[rows, :].astype(F32)
        cum = c_ref[rows, :]
        k = gate_keys(a, gap_ref[...])
        q = [mixed[:, 96:120], extra[:, 32:72]]
        q = jnp.concatenate(q + q, axis=1)
        q = q * sigmoid(q) * (KD ** -0.5)
        qg = q * jnp.exp(cum)
        kn = (k * jnp.exp(-cum)).astype(BF16)
        qf = jnp.where(lane < 64, qg, 0.0).astype(BF16)
        qb = jnp.where(lane < 64, 0.0, qg).astype(BF16)
        qh = qg.astype(BF16)
        scores = jnp.where(lower, dot(qf, kn, NT), 0.0) + jnp.where(upper, dot(qb, kn, NT), 0.0)
        out = dot(scores.astype(BF16), v, NN)
        for h in range(2):
            part = slice(64 * h, 64 * (h + 1))
            to = slice(128 * b + 64 * h, 128 * b + 64 * (h + 1))
            out_ref[to, :] = out[part] + dot(qh[part], before_ref[2 * b + h], NT)
            qd_ref[to, :] = (qg[part] * jnp.exp(offset_ref[2 * b + h][0:1])).astype(BF16)
    pad[16 + n : 32 + n, :] = zeros
    taps = taps_ref[...]
    for blk in range(n // 64):
        acc = jnp.zeros((64, 32), F32)
        for j in range(31):
            acc += pad[64 * blk + j + 1 : 64 * blk + j + 65, :] * taps[j : j + 1, :]
        conv_ref[blk] = jnp.concatenate([acc[16 * q : 16 * (q + 1)] for q in range(4)], axis=1).astype(BF16)
        if blk == 0:
            edge_ref[0] = acc[0:16]
        if blk == n // 64 - 1:
            edge_ref[1] = acc[48:64]


def merge_kernel(z_ref, recv_ref, local_ref, qd_ref, conv_ref, edge_ref, taps_ref, send_ref):
    z = z_ref[0]
    heads = jnp.zeros((16, 128), F32)
    tails = jnp.zeros((16, 128), F32)
    for i in range(8):
        other = recv_ref[i, 32:48, :].astype(F32)
        tails = jnp.where(i == z - 1, other, tails)
        heads = jnp.where(i == z + 1, other, heads)
    zeros = jnp.zeros((16, 32), F32)
    before = jnp.concatenate([tails[:, 32:64], zeros], axis=0)
    after = jnp.concatenate([zeros, heads[:, 0:32]], axis=0)
    first, last = edge_ref[0], edge_ref[1]
    taps = taps_ref[...]
    for j in range(15):
        first += before[j + 1 : j + 17] * taps[j : j + 1, :]
        last += after[j + 1 : j + 17] * taps[16 + j : 17 + j, :]
    first = jnp.concatenate([first] * 4, axis=1).astype(BF16)
    last = jnp.concatenate([last] * 4, axis=1).astype(BF16)
    lane16 = lanes(16)
    fwd = lanes(64) < 64
    fwd1 = lanes(1) < 64
    states, decays = [], []
    for i in range(8):
        packed = recv_ref[i, 0:32, :].astype(F32)
        states.append((packed, pltpu.roll(packed, 64, 1)))
        parts = recv_ref[i, 32:48, :].astype(F32)
        both = parts[0:8] + jnp.concatenate([parts[1:8], parts[0:1]], axis=0)
        decays.append((pltpu.roll(both, 64, 1)[0:1], both[0:1]))
    s = jnp.zeros((64, 128), F32)
    for i in range(8):
        j = 7 - i
        sc_f = jnp.concatenate([states[i][0], states[i][1]], axis=0)
        sc_b = jnp.concatenate([states[j][1], states[j][0]], axis=0)
        sc = jnp.where(fwd, sc_f, sc_b)
        dec = jnp.where(fwd1, decays[i][0], decays[j][1])
        pass_f = jnp.where(i < z, 1, 0)
        pass_b = jnp.where(j > z, 1, 0)
        passed = jnp.where(fwd, pass_f, pass_b) > 0
        s = jnp.where(passed, s * dec + sc, s)
    full = s.astype(BF16)
    for blk in range(16):
        rows = slice(64 * blk, 64 * (blk + 1))
        out = local_ref[rows, :] + dot(qd_ref[rows, :], full, NT)
        send_ref[blk, :32, :] = jnp.concatenate([out[0:32], out[32:64]], axis=1).astype(BF16)
        packed = conv_ref[blk]
        if blk == 0:
            packed = jnp.where(lane16 < 32, first, packed)
        if blk == 15:
            packed = jnp.where(lane16 >= 96, last, packed)
        send_ref[blk, 32:, :] = packed


def output_kernel(
    recv_ref, rec_gain_ref, conv_gain_ref, w0_ref, w_hbm, out_ref, act, w1_ref, sem
):
    copy = pltpu.make_async_copy(w_hbm.at[1], w1_ref, sem)
    copy.start()
    for c in range(2):
        for h in range(2):
            low, high = [
                recv_ref[(4 * h + v) * 2 + c, :32, :].astype(F32)
                + recv_ref[(4 * h + 2 + v) * 2 + c, :32, :].astype(F32)
                for v in range(2)
            ]
            left = lanes(32) < 64
            rec = jnp.concatenate(
                [
                    jnp.where(left, low, pltpu.roll(high, 64, 1)),
                    jnp.where(left, pltpu.roll(low, 64, 1), high),
                ],
                axis=0,
            )
            rec = rec * lax.rsqrt(jnp.mean(rec * rec, axis=1, keepdims=True) + EPS)
            rec = rec * rec_gain_ref[2 * c + h : 2 * c + h + 1, :]
            at = 128 * (4 * c + h)
            act[:, at : at + 128] = rec.astype(BF16)
    lane = lanes(16) // 32
    blocks = []
    for c in range(2):
        for m in range(2):
            parts = [recv_ref[(4 * m + q) * 2 + c, 32:48, :].astype(F32) for q in range(4)]
            groups = []
            for g in range(4):
                value = jnp.zeros((16, 128), F32)
                for q in range(4):
                    moved = parts[q] if q == g else pltpu.roll(parts[q], (32 * (q - g)) % 128, 1)
                    value = jnp.where(lane == q, moved, value)
                groups.append(value)
            blocks.append(jnp.concatenate(groups, axis=0))
    total = sum(jnp.sum(b, axis=1, keepdims=True) for b in blocks)
    square = sum(jnp.sum(b * b, axis=1, keepdims=True) for b in blocks)
    mean = total / 512.0
    scale = lax.rsqrt(square / 512.0 - mean * mean + EPS)
    for c in range(2):
        for m in range(2):
            n = 2 * c + m
            y = (blocks[n] - mean) * scale * conv_gain_ref[n : n + 1, :]
            at = 128 * (4 * c + 2 + m)
            act[:, at : at + 128] = (y * sigmoid(y)).astype(BF16)

    half = dot(act[:, 0:512], w0_ref[...], NT)
    copy.wait()
    out_ref[...] = (half + dot(act[:, 512:1024], w1_ref[...], NT)).astype(BF16)


def load_kernel(w_hbm, w_ref, sem):
    copy = pltpu.make_async_copy(w_hbm.at[0], w_ref, sem)
    copy.start()
    copy.wait()


def near(x):
    return pltpu.with_memory_space_constraint(x, pltpu.VMEM)


def kept(shape, dtype):
    return pltpu.VMEM(shape, dtype)


def body(
    tokens, norm_gain, rec_query, rec_input, rec_forward, rec_backward, forget_gap, log_decay,
    rec_gain, conv_value, conv_gate, conv_kernel, conv_gain, out_rec, out_conv,
):
    y, z = lax.axis_index(Y), lax.axis_index(Z)

    gap = lax.dynamic_index_in_dim(forget_gap.reshape(2, 4, 64), y // 2, 1, keepdims=False)
    gap = gap.reshape(1, 128)
    taps = lax.dynamic_index_in_dim(conv_kernel.reshape(31, 8, 32), y, 1, keepdims=False)
    taps = jnp.pad(taps.astype(F32), ((0, 1), (0, 0)))
    normed, first = pl.pallas_call(
        start_kernel,
        out_shape=[kept((64, 2048), BF16), kept((8, 32, 896), BF16)],
        name="start",
    )(
        tokens[0], norm_gain.reshape(1, 2048), rec_forward, rec_backward, rec_query, conv_value,
        conv_gate, rec_input, log_decay[0], out_rec.T, out_conv.T,
    )
    seq = lax.all_gather(normed, (Y, C), axis=0, tiled=True)
    first = lax.all_to_all(first, Y, split_axis=0, concat_axis=0, tiled=True)
    second, second2, out_cols, decays, gap, taps = pl.pallas_call(
        second_kernel,
        out_shape=[
            kept((248, 256), BF16),
            kept((8, 72, 256), BF16),
            jax.ShapeDtypeStruct((256, 512), BF16),
            kept((8, 2, 128), F32),
            kept((1, 128), F32),
            kept((32, 32), F32),
        ],
        name="second",
    )(near(first), near(gap), near(taps))
    weights2 = lax.all_to_all(second2, Z, split_axis=0, concat_axis=0, tiled=True)
    weights = lax.all_gather(second, Z, axis=0)
    out_w = lax.all_gather(out_cols, (C, Z), axis=0, tiled=True).reshape(2, 2048, 512)

    gains = lax.all_gather(jnp.stack([rec_gain, conv_gain]), C)
    rec_gains = gains[:, 0].reshape(4, 128)
    conv_gains = gains[:, 1].reshape(4, 128)
    n = seq.shape[0]
    seq = pltpu.with_memory_space_constraint(seq, pltpu.HBM)
    weights2 = near(weights2)
    z = z.reshape(1).astype(jnp.int32)
    pre_a, pre_v, cum, sent, before, offset = pl.pallas_call(
        states_kernel,
        in_specs=[pl.BlockSpec(memory_space=pltpu.SMEM), pl.BlockSpec(memory_space=pltpu.HBM)]
        + [pl.BlockSpec(memory_space=pltpu.VMEM)] * 4,
        out_shape=[
            kept((n, 128), BF16),
            kept((n, 128), BF16),
            kept((n, 128), F32),
            kept((8, 48, 128), BF16),
            kept((16, 64, 128), BF16),
            kept((16, 8, 128), F32),
        ],
        scratch_shapes=[
            pltpu.VMEM((n, 2048), BF16), pltpu.SemaphoreType.DMA((n // TILE,)),
            pltpu.VMEM((16, 64, 128), F32), pltpu.VMEM((16, 8, 128), F32),
        ],
        compiler_params=SMALL, name="states",
    )(z, seq, near(weights), weights2, near(decays), near(gap))

    arrived = lax.all_to_all(sent, Z, split_axis=0, concat_axis=0, tiled=True)
    local, decayed, convolved, edges = pl.pallas_call(
        local_kernel,
        out_shape=[
            kept((n, 64), F32),
            kept((n, 128), BF16),
            kept((16, 16, 128), BF16),
            kept((2, 16, 32), F32),
        ],
        in_specs=[pl.BlockSpec(memory_space=pltpu.HBM)]
        + [pl.BlockSpec(memory_space=pltpu.VMEM)] * 8,
        scratch_shapes=[
            pltpu.VMEM((n, 2048), BF16), pltpu.SemaphoreType.DMA((n // TILE,)),
            pltpu.VMEM((n + 32, 32), F32),
        ],
        compiler_params=SMALL, name="local",
    )(
        seq, weights2, near(pre_a), near(pre_v), near(cum), near(gap), near(before), near(offset),
        near(taps),
    )
    merged = pl.pallas_call(
        merge_kernel,
        in_specs=[pl.BlockSpec(memory_space=pltpu.SMEM)]
        + [pl.BlockSpec(memory_space=pltpu.VMEM)] * 6,
        out_shape=kept((16, 48, 128), BF16),
        compiler_params=SMALL, name="merge",
    )(z, near(arrived), near(local), near(decayed), near(convolved), near(edges), near(taps))
    mine = lax.all_to_all(merged, (Y, C), split_axis=0, concat_axis=0, tiled=True)
    out_w = pltpu.with_memory_space_constraint(out_w, pltpu.HBM)
    out_w0 = pl.pallas_call(
        load_kernel,
        in_specs=[pl.BlockSpec(memory_space=pltpu.HBM)],
        out_shape=kept((2048, 512), BF16),
        scratch_shapes=[pltpu.SemaphoreType.DMA],
        compiler_params=SMALL,
        name="load",
    )(out_w)
    mixed = pl.pallas_call(
        output_kernel,
        in_specs=[pl.BlockSpec(memory_space=pltpu.VMEM)] * 4
        + [pl.BlockSpec(memory_space=pltpu.HBM)],
        out_shape=jax.ShapeDtypeStruct((64, 2048), BF16),
        scratch_shapes=[
            pltpu.VMEM((64, 1024), BF16), pltpu.VMEM((2048, 512), BF16), pltpu.SemaphoreType.DMA
        ],
        compiler_params=SMALL, name="output",
    )(near(mine), rec_gains, conv_gains, near(out_w0), out_w)
    return mixed[None]


def solution(mesh):
    finer = Mesh(
        mesh.devices.reshape(8, 8, mesh.shape["fs"], mesh.shape["tp"]), (Z, Y, X, C)
    )
    sp, sp_tp = (Z, Y), (Z, Y, C)
    row = P(sp, C)
    placed = (
        P(X, sp_tp, None), P(), row, row, row, row, P(None, C), P(X, None, C, sp), P(C),
        row, row, P(None, C), P(C), P(C, sp), P(C, sp),
    )
    return jax.shard_map(
        body, mesh=finer, in_specs=placed, out_specs=P(X, sp_tp, None), check_vma=False
    )
```

profile of v0, /device:TPU:1, one launch (start us, length us, event | category | flops | bytes accessed | tf_op | source)
XLA Modules:
  0.0 123.4 jit_solution(1919800942506328820)
XLA Ops:
  6.5 0.0 all-gather.6.cloned.1.call-start
  6.5 2.1 %start.1 = (bf16[64,2048]{1,0:T(8,128)(2,1)}, bf16[8,32,896]{2,1,0:T(8,128)(2,1)}) custom-call(bf16[64,2048]{1,0:T(8,128)(2,1)} %bitcast.26, f32[1,2048]{1,0:T(1,128)} %bitcast.30, bf16[32,256]{1,0:T(8,128)(2,1)} %rf_ref.1, bf16[32,256]{1,0:T(8,128)(2,1)} %rb_ref.1, bf16[32,256]{1,0:T(8,128)(2,1)} %rq_ref.1, bf16[32,256]{1,0:T(8,128)(2,1)} %cv_ref.1, ...), custom_call_target="tpu_custom_call" | custom-call | tf_op jit(solution)/shard_map/start/pallas_call | solution.py:412
  8.6 0.0 all-gather.6.cloned.1.call-update
  8.7 7.7 %all-to-all-start = ((bf16[8,32,896]{2,1,0:T(8,128)(2,1)}), bf16[8,32,896]{2,1,0:T(8,128)(2,1)S(1)}, u32[]{:S(2)}, u32[]{:S(2)}) async-start(bf16[8,32,896]{2,1,0:T(8,128)(2,1)} %get-tuple-element.24), calls=%async_computation | async-start | bytes 917504 | tf_op jit(solution)/shard_map/all_to_all | solution.py:421
  16.3 0.0 all-gather.8.cloned.1.call-start
  16.4 0.8 reshape.23
  17.1 0.1 reshape.24.gap_ref
  17.2 0.8 reshape.25
  18.1 11.3 %all-to-all-done.first_ref = bf16[8,32,896]{2,1,0:T(8,128)(2,1)S(1)} async-done(((bf16[8,32,896]{2,1,0:T(8,128)(2,1)}), bf16[8,32,896]{2,1,0:T(8,128)(2,1)S(1)}, u32[]{:S(2)}, u32[]{:S(2)}) %all-to-all-start) | async-done | bytes 458784 | tf_op jit(solution)/shard_map/all_to_all | solution.py:421
  29.4 1.0 second.1
  30.4 0.0 all-gather.8.cloned.1.call-update
  30.4 14.1 %all-to-all-start.1 = ((bf16[8,72,256]{2,1,0:T(8,128)(2,1)}), bf16[8,72,256]{2,1,0:T(8,128)(2,1)S(1)}, u32[]{:S(2)}, u32[]{:S(2)}) async-start(bf16[8,72,256]{2,1,0:T(8,128)(2,1)} %get-tuple-element.26), calls=%async_computation.1 | async-start | bytes 589824 | tf_op jit(solution)/shard_map/all_to_all | solution.py:434
  44.6 26.5 %all-gather = bf16[1984,256]{1,0:T(8,128)(2,1)S(1)} all-gather(bf16[248,256]{1,0:T(8,128)(2,1)S(1)} %get-tuple-element.25), channel_id=2, replica_groups=mesh['sp_0'=8,'sp_1'=8,'fs'=4,'tp'=2] {'sp_0'}, dimensions={0}, use_global_device_ids=true | all-gather | bytes 1142784 | tf_op jit(solution)/shard_map/all_gather | solution.py:435
  71.0 0.0 all-to-all-done.1.w2_ref
  71.0 0.0 all-gather.6.cloned.1.call-done.x_hbm
  71.0 6.1 %states.1 = (bf16[1024,128]{1,0:T(8,128)(2,1)S(1)}, bf16[1024,128]{1,0:T(8,128)(2,1)S(1)}, f32[1024,128]{1,0:T(8,128)S(1)}, bf16[8,48,128]{2,1,0:T(8,128)(2,1)},...) custom-call(s32[1]{0:T(128)} %bitcast.z_ref, bf16[1024,2048]{1,0:T(8,128)(2,1)} %all-gather.6.cloned.1.call-done.x_hbm, ...), custom_call_target="tpu_custom_call" | custom-call | tf_op jit(solution)/shard_map/states/pallas_call | solution.py:445
  77.2 0.0 copy-start
  77.2 0.0 copy-start.1
  77.2 5.6 %all-to-all-start.2 = ((bf16[8,48,128]{2,1,0:T(8,128)(2,1)}), bf16[8,48,128]{2,1,0:T(8,128)(2,1)S(1)}, u32[]{:S(2)}, u32[]{:S(2)}) async-start(bf16[8,48,128]{2,1,0:T(8,128)(2,1)} %get-tuple-element.29), calls=%async_computation.2 | async-start | bytes 196608 | tf_op jit(solution)/shard_map/all_to_all | solution.py:464
  82.8 7.1 %local.1 = (f32[1024,64]{1,0:T(8,128)S(1)}, bf16[1024,128]{1,0:T(8,128)(2,1)S(1)}, bf16[16,16,128]{2,1,0:T(8,128)(2,1)S(1)}, f32[2,16,32]{2,1,0:T(8,128)S(1)}) custom-call(bf16[1024,2048]{1,0:T(8,128)(2,1)} %all-gather.6.cloned.1.call-done.x_hbm, bf16[8,72,256]{2,1,0:T(8,128)(2,1)S(1)} %all-to-all-done.1.w2_ref, ...), custom_call_target="tpu_custom_call" | custom-call | tf_op jit(solution)/shard_map/local/pallas_call | solution.py:465
  89.9 0.5 all-to-all-done.2.recv_ref
  90.3 1.1 merge.1
  91.5 11.1 %all-to-all-start.3 = ((bf16[16,48,128]{2,1,0:T(8,128)(2,1)}), bf16[16,48,128]{2,1,0:T(8,128)(2,1)S(1)}, u32[]{:S(2)}, u32[]{:S(2)}) async-start(bf16[16,48,128]{2,1,0:T(8,128)(2,1)} %merge.1), calls=%async_computation.3 | async-start | bytes 393216 | tf_op jit(solution)/shard_map/all_to_all | solution.py:491
  102.6 0.0 copy-done
  102.6 0.0 copy-done.1
  102.6 1.8 %all-gather.2 = f32[2,2,256]{2,1,0:T(2,128)S(1)} all-gather(f32[1,2,256]{2,1,0:T(2,128)S(1)} %maximum_bitcast_fusion), channel_id=3, replica_groups=mesh['sp_0'=8,'sp_1'=8,'fs'=4,'tp'=2] {'tp'}, dimensions={0}, use_global_device_ids=true | all-gather | bytes 6144 | tf_op jit(solution)/shard_map/all_gather | solution.py:438
  104.5 3.7 %all-gather.8.cloned.1.call-done = bf16[4096,512]{1,0:T(8,128)(2,1)} async-done(((bf16[256,512]{1,0:T(8,128)(2,1)}), bf16[4096,512]{1,0:T(8,128)(2,1)}) %all-gather.8.cloned.1.call-update) | async-done | bytes 4194320 | tf_op jit(solution)/shard_map/all_gather | solution.py:436
  108.2 1.6 %load.1.w0_ref = bf16[2048,512]{1,0:T(8,128)(2,1)S(1)} custom-call(bf16[2,2048,512]{2,1,0:T(8,128)(2,1)} %bitcast.24), custom_call_target="tpu_custom_call" | custom-call | tf_op jit(solution)/shard_map/load/pallas_call | solution.py:493
  109.8 3.0 %all-to-all-done.3.recv_ref = bf16[16,48,128]{2,1,0:T(8,128)(2,1)S(1)} async-done(((bf16[16,48,128]{2,1,0:T(8,128)(2,1)}), bf16[16,48,128]{2,1,0:T(8,128)(2,1)S(1)}, u32[]{:S(2)}, u32[]{:S(2)}) %all-to-all-start.3) | async-done | bytes 196640 | tf_op jit(solution)/shard_map/all_to_all | solution.py:491
  112.9 3.7 %output.1 = bf16[64,2048]{1,0:T(8,128)(2,1)} custom-call(bf16[16,48,128]{2,1,0:T(8,128)(2,1)S(1)} %all-to-all-done.3.recv_ref, f32[4,128]{1,0:T(4,128)S(1)} %bitcast.23, f32[4,128]{1,0:T(4,128)S(1)} %bitcast.22, bf16[2048,512]{1,0:T(8,128)(2,1)S(1)} %load.1.w0_ref, bf16[2,2048,512]{2,1,0:T(8,128)(2,1)} %bitcast.25), custom_call_target="tpu_custom_call" | custom-call | tf_op jit(solution)/shard_map/output/pallas_call | solution.py:501
  (6 shorter events, 0.1 us)
Async XLA Ops:
  6.5 64.5 %all-gather.6.cloned.1.call-start = ((), (), s32[]{:S(2)}) async-start(), calls=%async_computation.4 | async-start | bytes 4456448 | tf_op jit(solution)/shard_map/all_gather | solution.py:420
  8.7 20.8 %all-to-all-start = ((bf16[8,32,896]{2,1,0:T(8,128)(2,1)}), bf16[8,32,896]{2,1,0:T(8,128)(2,1)S(1)}, u32[]{:S(2)}, u32[]{:S(2)}) async-start(bf16[8,32,896]{2,1,0:T(8,128)(2,1)} %get-tuple-element.24), calls=%async_computation | async-start | bytes 917504 | tf_op jit(solution)/shard_map/all_to_all | solution.py:421
  16.3 91.9 %all-gather.8.cloned.1.call-start = ((), (), s32[]{:S(2)}) async-start(), calls=%async_computation.5 | async-start | bytes 4456448 | tf_op jit(solution)/shard_map/all_gather | solution.py:436
  30.4 40.6 %all-to-all-start.1 = ((bf16[8,72,256]{2,1,0:T(8,128)(2,1)}), bf16[8,72,256]{2,1,0:T(8,128)(2,1)S(1)}, u32[]{:S(2)}, u32[]{:S(2)}) async-start(bf16[8,72,256]{2,1,0:T(8,128)(2,1)} %get-tuple-element.26), calls=%async_computation.1 | async-start | bytes 589824 | tf_op jit(solution)/shard_map/all_to_all | solution.py:434
  77.2 25.5 %copy-start = (f32[256]{0:T(256)S(1)}, f32[256]{0:T(256)}, u32[]{:S(2)}) copy-start(f32[256]{0:T(256)} %param.27) | copy-start | bytes 3076
  77.2 25.5 %copy-start.1 = (f32[256]{0:T(256)S(1)}, f32[256]{0:T(256)}, u32[]{:S(2)}) copy-start(f32[256]{0:T(256)} %param.23) | copy-start | bytes 3076
  77.2 13.2 %all-to-all-start.2 = ((bf16[8,48,128]{2,1,0:T(8,128)(2,1)}), bf16[8,48,128]{2,1,0:T(8,128)(2,1)S(1)}, u32[]{:S(2)}, u32[]{:S(2)}) async-start(bf16[8,48,128]{2,1,0:T(8,128)(2,1)} %get-tuple-element.29), calls=%async_computation.2 | async-start | bytes 196608 | tf_op jit(solution)/shard_map/all_to_all | solution.py:464
  91.5 21.4 %all-to-all-start.3 = ((bf16[16,48,128]{2,1,0:T(8,128)(2,1)}), bf16[16,48,128]{2,1,0:T(8,128)(2,1)S(1)}, u32[]{:S(2)}, u32[]{:S(2)}) async-start(bf16[16,48,128]{2,1,0:T(8,128)(2,1)} %merge.1), calls=%async_computation.3 | async-start | bytes 393216 | tf_op jit(solution)/shard_map/all_to_all | solution.py:491
Sparse Core Ops, SparseCore 0:
  9.4 50.2 all-gather.5
  61.9 46.3 all-gather.7
where the time goes:
time: 124 us; the launch traced here: 123 us
  starting transfers between devices  38.6 us (31%)
  blocking collectives  28.3 us (23%)
  Pallas kernels  22.7 us (18%)
  waiting for transfers between devices  18.6 us (15%)
  between operations  13.5 us (11%)
  local copies, waits for them, and re-layouts  1.72 us (1%)
    all_gather x1, blocking collectives, body(): weights = lax.all_gather(second, Z, axis=0)  26.5 us
    all_to_all x1, starting transfers between devices, body(): lax.all_to_all(second2, Z, split_axis=0, concat_axis=0, tiled=True)  14.1 us
    all_to_all x1, waiting for transfers between devices, body(): first = lax.all_to_all(first, Y, split_axis=0, concat_axis=0, tiled=True)  11.3 us
    all_to_all x1, starting transfers between devices, body(): lax.all_to_all(merged, (Y, C), split_axis=0, concat_axis=0, tiled=True)  11.1 us
    all_to_all x1, starting transfers between devices, body(): first = lax.all_to_all(first, Y, split_axis=0, concat_axis=0, tiled=True)  7.65 us
    pallas_call x1, Pallas kernels, body(): pl.pallas_call(local_kernel, out_shape=[kept((n, 64), F32), kept((n, 128)...  7.05 us
    pallas_call x1, Pallas kernels, body(): pl.pallas_call(states_kernel, in_specs=[pl.BlockSpec(memory_space=pltpu.S...  6.14 us
    all_to_all x1, starting transfers between devices, body(): arrived = lax.all_to_all(sent, Z, split_axis=0, concat_axis=0, tiled=True)  5.63 us
  transfers between devices with their start and end apart: 6, of which 4 were waited for; matrix products, arithmetic and copies ran while one was open for 1% of the time, Pallas kernels for 14%

commit v1 on v0

--- a/solution.py
+++ b/solution.py
@@ -8,7 +8,7 @@
 
 KD = 128
 BLOCK = 64
-TILE = 512
+TILE = 256
 SMALL = pltpu.CompilerParams(vmem_limit_bytes=24 * 1024 * 1024)
 EPS = 1e-06
 Z, Y, X, C = "sp_0", "sp_1", "fs", "tp"
@@ -180,11 +180,14 @@
                 gates((t - 1) * (rows // 128) + b)
         a_ref[at, :] = acc[:, :128].astype(BF16)
         v_ref[at, :] = jnp.concatenate([acc[:, 128:], jnp.zeros((rows, 8), F32)], axis=1).astype(BF16)
-    ends = []
-    for at in (slice(0, 16), slice(total - 16, total)):
-        gate = rounded(project(x_ref, w2_ref, at, 72)[:, 0:32])
-        ends.append(v_ref[at, :].astype(F32)[:, 64:96] * sigmoid(gate))
-    head, last = ends
+    both = jnp.zeros((32, 32), F32)
+    for k in range(8):
+        cols = slice(256 * k, 256 * (k + 1))
+        xk = jnp.concatenate([x_ref[0:16, cols], x_ref[total - 16 : total, cols]], axis=0)
+        both += dot(xk, w2_ref[k, 0:32, :], NT)
+    both = sigmoid(rounded(both))
+    head = v_ref[0:16, :].astype(F32)[:, 64:96] * both[0:16]
+    last = v_ref[total - 16 : total, :].astype(F32)[:, 64:96] * both[16:32]
     for b in range(total // 128 - rows // 128, total // 128):
         gates(b)
 

time: 124 us -> 123 us (level)
  transfers between devices with their start and end apart: 6 -> 6, of which waited for: 4 -> 4; matrix products, arithmetic and copies ran while one was open for 1% -> 1% of each run, Pallas kernels for 14% -> 13%
where the time goes in v1:
time: 123 us
  starting transfers between devices  38.2 us (31%)
  blocking collectives  28.3 us (23%)
  Pallas kernels  22.3 us (18%)
  waiting for transfers between devices  18.8 us (15%)
  between operations  13.5 us (11%)
  local copies, waits for them, and re-layouts  1.72 us (1%)
    all_gather x1, blocking collectives, body(): weights = lax.all_gather(second, Z, axis=0)  26.5 us
    all_to_all x1, starting transfers between devices, body(): lax.all_to_all(second2, Z, split_axis=0, concat_axis=0, tiled=True)  14.1 us
    all_to_all x1, waiting for transfers between devices, body(): first = lax.all_to_all(first, Y, split_axis=0, concat_axis=0, tiled=True)  11.3 us
    all_to_all x1, starting transfers between devices, body(): lax.all_to_all(merged, (Y, C), split_axis=0, concat_axis=0, tiled=True)  10.9 us
    all_to_all x1, starting transfers between devices, body(): first = lax.all_to_all(first, Y, split_axis=0, concat_axis=0, tiled=True)  7.65 us
    pallas_call x1, Pallas kernels, body(): pl.pallas_call(local_kernel, out_shape=[kept((n, 64), F32), kept((n, 128)...  7.26 us
    pallas_call x1, Pallas kernels, body(): pl.pallas_call(states_kernel, in_specs=[pl.BlockSpec(memory_space=pltpu.S...  5.55 us
    all_to_all x1, starting transfers between devices, body(): arrived = lax.all_to_all(sent, Z, split_axis=0, concat_axis=0, tiled=True)  5.49 us
  transfers between devices with their start and end apart: 6, of which 4 were waited for; matrix products, arithmetic and copies ran while one was open for 1% of the time, Pallas kernels for 13%

profile of v1, /device:TPU:1, one launch (start us, length us, event | category | flops | bytes accessed | tf_op | source)
XLA Modules:
  0.0 122.9 jit_solution(12565184671791194592)
XLA Ops:
  6.5 0.0 all-gather.6.cloned.1.call-start
  6.5 2.1 %start.1 = (bf16[64,2048]{1,0:T(8,128)(2,1)}, bf16[8,32,896]{2,1,0:T(8,128)(2,1)}) custom-call(bf16[64,2048]{1,0:T(8,128)(2,1)} %bitcast.26, f32[1,2048]{1,0:T(1,128)} %bitcast.30, bf16[32,256]{1,0:T(8,128)(2,1)} %rf_ref.1, bf16[32,256]{1,0:T(8,128)(2,1)} %rb_ref.1, bf16[32,256]{1,0:T(8,128)(2,1)} %rq_ref.1, bf16[32,256]{1,0:T(8,128)(2,1)} %cv_ref.1, ...), custom_call_target="tpu_custom_call" | custom-call | tf_op jit(solution)/shard_map/start/pallas_call | solution.py:415
  8.6 0.0 all-gather.6.cloned.1.call-update
  8.7 7.7 %all-to-all-start = ((bf16[8,32,896]{2,1,0:T(8,128)(2,1)}), bf16[8,32,896]{2,1,0:T(8,128)(2,1)S(1)}, u32[]{:S(2)}, u32[]{:S(2)}) async-start(bf16[8,32,896]{2,1,0:T(8,128)(2,1)} %get-tuple-element.24), calls=%async_computation | async-start | bytes 917504 | tf_op jit(solution)/shard_map/all_to_all | solution.py:424
  16.3 0.0 all-gather.8.cloned.1.call-start
  16.4 0.8 reshape.23
  17.1 0.1 reshape.24.gap_ref
  17.2 0.8 reshape.25
  18.1 11.3 %all-to-all-done.first_ref = bf16[8,32,896]{2,1,0:T(8,128)(2,1)S(1)} async-done(((bf16[8,32,896]{2,1,0:T(8,128)(2,1)}), bf16[8,32,896]{2,1,0:T(8,128)(2,1)S(1)}, u32[]{:S(2)}, u32[]{:S(2)}) %all-to-all-start) | async-done | bytes 458784 | tf_op jit(solution)/shard_map/all_to_all | solution.py:424
  29.4 1.0 second.1
  30.4 0.0 all-gather.8.cloned.1.call-update
  30.4 14.1 %all-to-all-start.1 = ((bf16[8,72,256]{2,1,0:T(8,128)(2,1)}), bf16[8,72,256]{2,1,0:T(8,128)(2,1)S(1)}, u32[]{:S(2)}, u32[]{:S(2)}) async-start(bf16[8,72,256]{2,1,0:T(8,128)(2,1)} %get-tuple-element.26), calls=%async_computation.1 | async-start | bytes 589824 | tf_op jit(solution)/shard_map/all_to_all | solution.py:437
  44.6 26.5 %all-gather = bf16[1984,256]{1,0:T(8,128)(2,1)S(1)} all-gather(bf16[248,256]{1,0:T(8,128)(2,1)S(1)} %get-tuple-element.25), channel_id=2, replica_groups=mesh['sp_0'=8,'sp_1'=8,'fs'=4,'tp'=2] {'sp_0'}, dimensions={0}, use_global_device_ids=true | all-gather | bytes 1142784 | tf_op jit(solution)/shard_map/all_gather | solution.py:438
  71.0 0.0 all-to-all-done.1.w2_ref
  71.0 0.0 all-gather.6.cloned.1.call-done.x_hbm
  71.0 5.5 %states.1 = (bf16[1024,128]{1,0:T(8,128)(2,1)S(1)}, bf16[1024,128]{1,0:T(8,128)(2,1)S(1)}, f32[1024,128]{1,0:T(8,128)S(1)}, bf16[8,48,128]{2,1,0:T(8,128)(2,1)},...) custom-call(s32[1]{0:T(128)} %bitcast.z_ref, bf16[1024,2048]{1,0:T(8,128)(2,1)} %all-gather.6.cloned.1.call-done.x_hbm, ...), custom_call_target="tpu_custom_call" | custom-call | tf_op jit(solution)/shard_map/states/pallas_call | solution.py:448
  76.6 0.0 copy-start
  76.6 0.0 copy-start.1
  76.6 5.5 %all-to-all-start.2 = ((bf16[8,48,128]{2,1,0:T(8,128)(2,1)}), bf16[8,48,128]{2,1,0:T(8,128)(2,1)S(1)}, u32[]{:S(2)}, u32[]{:S(2)}) async-start(bf16[8,48,128]{2,1,0:T(8,128)(2,1)} %get-tuple-element.29), calls=%async_computation.2 | async-start | bytes 196608 | tf_op jit(solution)/shard_map/all_to_all | solution.py:467
  82.1 7.3 %local.1 = (f32[1024,64]{1,0:T(8,128)S(1)}, bf16[1024,128]{1,0:T(8,128)(2,1)S(1)}, bf16[16,16,128]{2,1,0:T(8,128)(2,1)S(1)}, f32[2,16,32]{2,1,0:T(8,128)S(1)}) custom-call(bf16[1024,2048]{1,0:T(8,128)(2,1)} %all-gather.6.cloned.1.call-done.x_hbm, bf16[8,72,256]{2,1,0:T(8,128)(2,1)S(1)} %all-to-all-done.1.w2_ref, ...), custom_call_target="tpu_custom_call" | custom-call | tf_op jit(solution)/shard_map/local/pallas_call | solution.py:468
  89.4 0.6 all-to-all-done.2.recv_ref
  90.0 1.1 merge.1
  91.1 10.9 %all-to-all-start.3 = ((bf16[16,48,128]{2,1,0:T(8,128)(2,1)}), bf16[16,48,128]{2,1,0:T(8,128)(2,1)S(1)}, u32[]{:S(2)}, u32[]{:S(2)}) async-start(bf16[16,48,128]{2,1,0:T(8,128)(2,1)} %merge.1), calls=%async_computation.3 | async-start | bytes 393216 | tf_op jit(solution)/shard_map/all_to_all | solution.py:494
  102.1 0.0 copy-done
  102.1 0.0 copy-done.1
  102.1 1.8 %all-gather.2 = f32[2,2,256]{2,1,0:T(2,128)S(1)} all-gather(f32[1,2,256]{2,1,0:T(2,128)S(1)} %maximum_bitcast_fusion), channel_id=3, replica_groups=mesh['sp_0'=8,'sp_1'=8,'fs'=4,'tp'=2] {'tp'}, dimensions={0}, use_global_device_ids=true | all-gather | bytes 6144 | tf_op jit(solution)/shard_map/all_gather | solution.py:441
  103.9 4.5 %all-gather.8.cloned.1.call-done = bf16[4096,512]{1,0:T(8,128)(2,1)} async-done(((bf16[256,512]{1,0:T(8,128)(2,1)}), bf16[4096,512]{1,0:T(8,128)(2,1)}) %all-gather.8.cloned.1.call-update) | async-done | bytes 4194320 | tf_op jit(solution)/shard_map/all_gather | solution.py:439
  108.4 1.6 %load.1.w0_ref = bf16[2048,512]{1,0:T(8,128)(2,1)S(1)} custom-call(bf16[2,2048,512]{2,1,0:T(8,128)(2,1)} %bitcast.24), custom_call_target="tpu_custom_call" | custom-call | tf_op jit(solution)/shard_map/load/pallas_call | solution.py:496
  110.1 2.3 %all-to-all-done.3.recv_ref = bf16[16,48,128]{2,1,0:T(8,128)(2,1)S(1)} async-done(((bf16[16,48,128]{2,1,0:T(8,128)(2,1)}), bf16[16,48,128]{2,1,0:T(8,128)(2,1)S(1)}, u32[]{:S(2)}, u32[]{:S(2)}) %all-to-all-start.3) | async-done | bytes 196640 | tf_op jit(solution)/shard_map/all_to_all | solution.py:494
  112.3 3.7 %output.1 = bf16[64,2048]{1,0:T(8,128)(2,1)} custom-call(bf16[16,48,128]{2,1,0:T(8,128)(2,1)S(1)} %all-to-all-done.3.recv_ref, f32[4,128]{1,0:T(4,128)S(1)} %bitcast.23, f32[4,128]{1,0:T(4,128)S(1)} %bitcast.22, bf16[2048,512]{1,0:T(8,128)(2,1)S(1)} %load.1.w0_ref, bf16[2,2048,512]{2,1,0:T(8,128)(2,1)} %bitcast.25), custom_call_target="tpu_custom_call" | custom-call | tf_op jit(solution)/shard_map/output/pallas_call | solution.py:504
  (6 shorter events, 0.1 us)
Async XLA Ops:
  6.5 64.5 %all-gather.6.cloned.1.call-start = ((), (), s32[]{:S(2)}) async-start(), calls=%async_computation.4 | async-start | bytes 4456448 | tf_op jit(solution)/shard_map/all_gather | solution.py:423
  8.7 20.8 %all-to-all-start = ((bf16[8,32,896]{2,1,0:T(8,128)(2,1)}), bf16[8,32,896]{2,1,0:T(8,128)(2,1)S(1)}, u32[]{:S(2)}, u32[]{:S(2)}) async-start(bf16[8,32,896]{2,1,0:T(8,128)(2,1)} %get-tuple-element.24), calls=%async_computation | async-start | bytes 917504 | tf_op jit(solution)/shard_map/all_to_all | solution.py:424
  16.3 92.1 %all-gather.8.cloned.1.call-start = ((), (), s32[]{:S(2)}) async-start(), calls=%async_computation.5 | async-start | bytes 4456448 | tf_op jit(solution)/shard_map/all_gather | solution.py:439
  30.4 40.6 %all-to-all-start.1 = ((bf16[8,72,256]{2,1,0:T(8,128)(2,1)}), bf16[8,72,256]{2,1,0:T(8,128)(2,1)S(1)}, u32[]{:S(2)}, u32[]{:S(2)}) async-start(bf16[8,72,256]{2,1,0:T(8,128)(2,1)} %get-tuple-element.26), calls=%async_computation.1 | async-start | bytes 589824 | tf_op jit(solution)/shard_map/all_to_all | solution.py:437
  76.6 25.5 %copy-start = (f32[256]{0:T(256)S(1)}, f32[256]{0:T(256)}, u32[]{:S(2)}) copy-start(f32[256]{0:T(256)} %param.27) | copy-start | bytes 3076
  76.6 25.5 %copy-start.1 = (f32[256]{0:T(256)S(1)}, f32[256]{0:T(256)}, u32[]{:S(2)}) copy-start(f32[256]{0:T(256)} %param.23) | copy-start | bytes 3076
  76.6 13.4 %all-to-all-start.2 = ((bf16[8,48,128]{2,1,0:T(8,128)(2,1)}), bf16[8,48,128]{2,1,0:T(8,128)(2,1)S(1)}, u32[]{:S(2)}, u32[]{:S(2)}) async-start(bf16[8,48,128]{2,1,0:T(8,128)(2,1)} %get-tuple-element.29), calls=%async_computation.2 | async-start | bytes 196608 | tf_op jit(solution)/shard_map/all_to_all | solution.py:467
  91.1 21.2 %all-to-all-start.3 = ((bf16[16,48,128]{2,1,0:T(8,128)(2,1)}), bf16[16,48,128]{2,1,0:T(8,128)(2,1)S(1)}, u32[]{:S(2)}, u32[]{:S(2)}) async-start(bf16[16,48,128]{2,1,0:T(8,128)(2,1)} %merge.1), calls=%async_computation.3 | async-start | bytes 393216 | tf_op jit(solution)/shard_map/all_to_all | solution.py:494
Sparse Core Ops, SparseCore 0:
  9.4 50.2 all-gather.5
  61.9 46.5 all-gather.7
